TPU v7x, 128 devices: a whole 4x4x4 slice. The times are simulated.
128 devices in a mesh: rep: 2 (over z_hi), fs: 32 (over z_lo, y, x), tp: 2 (over core).
Axes of the slice: x: 4, y: 4, z: 4 (z_hi: 2, z_lo: 2; z = z_hi * 2 + z_lo), core: 2. Of those that a mesh axis runs over, the one named last changes fastest.
Arguments:
- inputs: bfloat16 [32768, 1024], P(('rep', 'fs', 'tp')), may hold values from -6 to 6
- up_proj: bfloat16 [1024, 4096], P('fs', 'tp'), may hold values from -0.1875 to 0.1875
- down_proj: bfloat16 [4096, 1024], P('tp', 'fs'), may hold values from -0.09375 to 0.09375
- out_cotangent: bfloat16 [32768, 1024], P(('rep', 'fs', 'tp')), may hold values from -24 to 24
Outputs:
- grad_inputs: bfloat16 [32768, 1024], P(('rep', 'fs', 'tp'))
- grad_up: float32 [1024, 4096], P('fs', 'tp')
- grad_down: float32 [4096, 1024], P('tp', 'fs')
- energy_up: float32 [1024], P('fs')
- energy_down: float32 [4096], P('tp')
All inputs are finite; a program needn't handle non-finite values.
Results may differ from a plain program's by a relative error of at most 0.001.
Values may be sent and summed in bfloat16 or wider, within the bound.
A program may use at most 128 MiB of HBM per device.

v0:
```python
import functools

import jax
import jax.numpy as jnp
from jax import lax
from jax.experimental import pallas as pl
from jax.experimental.pallas import tpu as pltpu
from jax.sharding import PartitionSpec as P

MESH = pl.DeviceIdType.MESH
GATHER = (
    (
        (2, 4, 0, 1, 3),
        (0, 3, 1, 2, 4),
        (1, 4, 0, 2, 3),
        (2, 3, 1, 0, 4),
        (4, 0, 2, 3, 1),
        (4, 3, 0, 1, 2),
        (1, 2, 3, 4, 0),
        (3, 1, 4, 0, 2),
    ),
    (
        (0, 4, 1, 3, 2),
        (3, 2, 0, 1, 4),
        (2, 4, 3, 1, 0),
        (1, 3, 2, 0, 4),
        (0, 1, 2, 4, 3),
        (2, 4, 3, 1, 0),
        (2, 1, 4, 0, 3),
        (3, 0, 4, 2, 1),
    ),
)
REDUCE = (
    (
        (4, 3, 0, 1, 2),
        (0, 1, 2, 4, 3),
        (2, 4, 3, 0, 1),
        (3, 1, 2, 0, 4),
        (4, 0, 1, 3, 2),
        (1, 2, 0, 4, 3),
        (3, 4, 2, 1, 0),
        (0, 3, 1, 2, 4),
    ),
    (
        (2, 1, 3, 4, 0),
        (4, 0, 2, 1, 3),
        (0, 4, 2, 1, 3),
        (4, 3, 1, 0, 2),
        (1, 4, 2, 3, 0),
        (4, 2, 3, 0, 1),
        (0, 3, 1, 4, 2),
        (2, 3, 1, 0, 4),
    ),
)
FIRST = (
    0, 10, 20, 40, 70, 30, 50, 60, 100, 110, 120, 130, 140, 170, 150, 160,
    1, 11, 41, 71, 61, 21, 31, 51, 101, 111, 141, 161, 171, 121, 131,
    151, 2, 12, 42, 72, 62, 22, 32, 52, 102, 122, 142, 132, -2, 162, 172,
    152, 112, 3, 13, 43, 63, 73, 53, 23, 33, 103, 143, 123, 173, 133, -3, -1,
    153, 163, 4, 14, 113, 74, 64, 24, 34, 44, 54,
)
THEN = (
    1010, 1011, 1012, 1013, 1100, 1000, 1101, 100, 110, 1001, 130, 150, 1102, 140, 120, 170,
    1002, 160, 101, 111, 1103, 10, 131, 1003, 0, 141, 151, 30, 20, 1201, 171, 161,
    121, 132, 40, 50, 11, 112, 1200, 102, 142, 1, 152, 60, 1301, 133, 172, 122,
    70, 162, 12, 31, 41, 51, 103, 1300, 153, 143, 21, 113, 134, 173, 123, 61,
    163, 2, 13, 71, 42, 154, 144, 52, 32, 114, 104, 22, 174, 124, 164, 3,
    14, 62, 43, 72, 53, 33, 23, 4, 1400, 63, 44, 1500, 54, 73, 34, 24,
    64, 1401, 74, 1402, 1310, 1311,
)
STEPS = 5
PARTS = 8
SPLIT = 2
SIZE = 2
UNITS = 16
BLOCKS = 8
HALF = (16, 8, 4, 2, 1)
SPAN = 240.0
SHIFT = 120.0


def encode(value, scale):
    code = jnp.exp2(jnp.abs(value) * (SPAN / scale) - SHIFT)
    return jnp.where(value < 0.0, -code, code).astype(jnp.bfloat16)


def decode(code, scale):
    code = code.astype(jnp.float32)
    size = (jnp.log2(jnp.abs(code)) + SHIFT) * (scale * (1.0 / SPAN))
    return jnp.where(code < 0.0, -size, size)


def scale_of(top):
    return (top * 1.01 + 1e-35).astype(jnp.bfloat16)


def bits_of(fs):
    z, y, x = fs // 16, (fs // 4) % 4, fs % 4
    return (z, (y % 2 + y // 2) % 2, y // 2, (x % 2 + x // 2) % 2, x // 2)


def partners_of(fs):
    z, y, x = fs // 16, (fs // 4) % 4, fs % 4
    return (
        fs + 16 - 32 * z,
        fs + 4 - 8 * (y % 2),
        fs + 12 - 8 * y,
        fs + 1 - 2 * (x % 2),
        fs + 3 - 2 * x,
    )


def remote(src, dst, send, recv, device):
    return pltpu.make_async_remote_copy(
        src_ref=src, dst_ref=dst, send_sem=send, recv_sem=recv, device_id=device, device_id_type=MESH
    )


def contract(left, right, left_dim, right_dim):
    return lax.dot_general(
        left, right, (((left_dim,), (right_dim,)), ((), ())), preferred_element_type=jnp.float32
    )


def kernel(
    factor,
    x_ref,
    c_ref,
    u_ref,
    d_ref,
    gin_ref,
    grad_ref,
    eup_ref,
    edn_ref,
    tok,
    tokt,
    wg,
    wn,
    pre,
    act,
    gpre,
    gbuf,
    sbuf,
    rbuf,
    part_in,
    pair_out,
    pair_in,
    outs,
    gin,
    ebuf,
    eup,
    load_s,
    tok_s,
    tok_r,
    fwd_s,
    fwd_r,
    sib_s,
    sib_r,
    g_s,
    g_r,
    r_s,
    r_r,
    rep_s,
    rep_r,
    pi_s,
    pi_r,
    li_s,
    li_r,
    e_s,
    e_r,
    eu_s,
    eu_r,
    out_s,
):
    rep, fs, tp = lax.axis_index("rep"), lax.axis_index("fs"), lax.axis_index("tp")
    mine = bits_of(fs)
    near = [{"fs": other} for other in partners_of(fs)]
    sibling = {"tp": 1 - tp}
    pair = {"rep": 1 - rep, "fs": partners_of(fs)[0]}
    twin = {"rep": 1 - rep}
    cross = {"rep": 1 - rep, "tp": 1 - tp}
    z, y, x = fs // 16, (fs // 4) % 4, fs % 4
    far_x = {"fs": fs + (x + 2) % 4 - x}
    far_y = {"fs": fs + 4 * ((y + 2) % 4 - y)}
    rows, width = x_ref.shape
    shard = u_ref.shape[0]
    hidden = u_ref.shape[1] // 2
    base = rep * hidden
    weights = (u_ref, d_ref)
    tokens = (x_ref, c_ref)
    pieces = 2
    chunk = rows // pieces
    half_rows = 2 * rows
    bw = 256
    blocks = hidden // bw
    all_parts = range(PARTS)
    f32, bf16 = jnp.float32, jnp.bfloat16

    flip = [(bit, 1 - bit) for bit in mine]
    tables = {}

    def slot(order, s):
        if order not in tables:
            place = {d: 2**k for k, d in enumerate(order)}
            high, low = [], []
            for v in range(8):
                bits = bits_of(4 * v)
                high.append(sum(flip[d][bits[d]] * place[d] for d in (0, 1, 2)))
            for v in range(4):
                bits = bits_of(v)
                low.append(sum(flip[d][bits[d]] * place[d] for d in (3, 4)))
            tables[order] = high, low
        high, low = tables[order]
        return high[s // 4] + low[s % 4]

    def home(m, p):
        return (m * PARTS + p) * 32 * SIZE

    def place_of(m, p):
        return (m * PARTS + p) * 32

    barrier = pltpu.get_barrier_semaphore()
    for device in near + [sibling, pair, twin, cross, far_x, far_y]:
        pl.semaphore_signal(barrier, inc=1, device_id=device, device_id_type=MESH)

    loads = []
    for m in range(2):
        loads.append(pltpu.make_async_copy(tokens[m], tok.at[m, pl.ds(0, rows)], load_s.at[16 + m]))
        for p in all_parts:
            columns = pl.ds(pl.multiple_of(base + p * 128, 128), 128)
            loads.append(
                pltpu.make_async_copy(
                    weights[m].at[:, columns], wg.at[place_of(m, p)], load_s.at[m * PARTS + p]
                )
            )
    for copy in loads:
        copy.start()
    for copy in loads:
        copy.wait()

    pl.semaphore_wait(barrier, STEPS + 6)

    pending = []

    def start(copy):
        copy.start()
        pending.append(copy)
        return copy

    def token_copy(m, q):
        return remote(
            tok.at[m, pl.ds(q * chunk, chunk)],
            tok.at[m, pl.ds(2 * rows + q * chunk, chunk)],
            tok_s.at[m, q],
            tok_r.at[m, q],
            pair,
        )

    def forward_copy(m, q):
        return remote(
            tok.at[m, pl.ds(2 * rows + q * chunk, chunk)],
            tok.at[m, pl.ds(3 * rows + q * chunk, chunk)],
            fwd_s.at[m, q],
            fwd_r.at[m, q],
            sibling,
        )

    def sibling_copy(m):
        return remote(tok.at[m, pl.ds(0, rows)], tok.at[m, pl.ds(rows, rows)], sib_s.at[m], sib_r.at[m], sibling)

    def gather_copy(m, p, k):
        n = 2**k
        return remote(
            wg.at[pl.ds(place_of(m, p), n)],
            wg.at[pl.ds(place_of(m, p) + n, n)],
            g_s.at[m * PARTS + p, k],
            g_r.at[m * PARTS + p, k],
            near[GATHER[m][p][k]],
        )

    def forward(m, q):
        token_copy(m, q).wait_recv()
        start(forward_copy(m, q))

    def transpose(m, g):
        tokt[m, :, g * rows : (g + 1) * rows] = tok[m, g * rows : (g + 1) * rows].T

    def unpack(m, p):
        for s in range(32):
            wn[m, s * shard : (s + 1) * shard, p * 128 : (p + 1) * 128] = wg[
                place_of(m, p) + slot(GATHER[m][p], s)
            ]

    def part_cols(j):
        return slice(j * bw, (j + 1) * bw)

    def forward_block(j):
        for h in range(2):
            part = slice(h * half_rows, (h + 1) * half_rows)
            kept = jnp.maximum(
                jnp.dot(tok[0, part], wn[0, :, part_cols(j)], preferred_element_type=f32), 0.0
            )
            pre[part, part_cols(j)] = kept
            act[part, part_cols(j)] = (kept * kept).astype(bf16)

    def back_block(j):
        for p in (2 * j, 2 * j + 1):
            gather_copy(1, p, STEPS - 1).wait_recv()
            unpack(1, p)
        for h in range(2):
            part = slice(h * half_rows, (h + 1) * half_rows)
            value = jnp.dot(tok[1, part], wn[1, :, part_cols(j)], preferred_element_type=f32)
            gpre[part, part_cols(j)] = (2.0 * pre[part, part_cols(j)] * value).astype(bf16)

    def room(m, p, k):
        before = sum(1 + HALF[i] * SIZE for i in range(k))
        return (m * PARTS + p) * (31 * SIZE + 5) + before

    def reduce_copy(m, p, k):
        place = pl.ds(room(m, p, k), 1 + HALF[k] * SIZE)
        return remote(
            sbuf.at[place],
            rbuf.at[place],
            r_s.at[m * PARTS + p, k],
            r_r.at[m * PARTS + p, k],
            near[REDUCE[m][p][STEPS - 1 - k]],
        )

    def chunks(count, size):
        step = min(count, 4) * size
        return count * size // step, step

    def highest(m, p, k):
        n = SIZE
        loops, step = chunks(HALF[k], n)
        at = home(m, p) + HALF[k] * n

        def some(i, top):
            return jnp.maximum(top, jnp.max(jnp.abs(gbuf[pl.ds(at + i * step, step)]), axis=0))

        return lax.fori_loop(0, loops, some, jnp.zeros((16, 128), f32))

    def send_sums(m, p, k, top):
        n = SIZE
        loops, step = chunks(HALF[k], n)
        at, to = home(m, p) + HALF[k] * n, room(m, p, k)
        coded = scale_of(top)
        sbuf[to] = coded
        scale = coded.astype(f32)

        def some(i, carry):
            sbuf[pl.ds(to + 1 + i * step, step)] = encode(gbuf[pl.ds(at + i * step, step)], scale)
            return carry

        lax.fori_loop(0, loops, some, 0)
        start(reduce_copy(m, p, k))

    def begin(m, p):
        send_sums(m, p, 0, highest(m, p, 0))

    def add_sums(m, p, k, first, count):
        n = SIZE
        loops, step = chunks(count, n)
        at, got = home(m, p) + first * n, room(m, p, k) + 1 + first * n
        scale = rbuf[room(m, p, k)].astype(f32)

        def some(i, top):
            place = pl.ds(at + i * step, step)
            value = gbuf[place] + decode(rbuf[pl.ds(got + i * step, step)], scale)
            gbuf[place] = value
            return jnp.maximum(top, jnp.max(jnp.abs(value), axis=0))

        return lax.fori_loop(0, loops, some, jnp.zeros((16, 128), f32))

    def reduce_step(m, p, k):
        reduce_copy(m, p, k).wait_recv()
        n = HALF[k + 1]
        top = add_sums(m, p, k, n, n)
        send_sums(m, p, k + 1, top)
        add_sums(m, p, k, 0, n)

    def weight_grad(m, right, j):
        tall = width // SPLIT
        for i in range(SPLIT):
            out = jnp.dot(
                tokt[m, i * tall : (i + 1) * tall, :], right[:, part_cols(j)], preferred_element_type=f32
            )
            for t in range(tall // shard):
                for e in range(2):
                    p = 2 * j + e
                    at = home(m, p) + slot(REDUCE[m][p], i * (tall // shard) + t) * SIZE
                    value = out[t * shard : (t + 1) * shard, e * 128 : (e + 1) * 128]
                    gbuf[pl.ds(at, SIZE)] = value.reshape(SIZE, 16, 128)
        begin(m, 2 * j)
        begin(m, 2 * j + 1)

    def share_copy(i):
        return remote(
            pre.at[pl.ds((1 + 2 * i) * rows, rows)], part_in.at[i], pi_s.at[i], pi_r.at[i], sibling
        )

    def pair_copy(q):
        return remote(pair_out.at[q], pair_in.at[q], li_s.at[q], li_r.at[q], pair)

    for m in range(2):
        for p in all_parts:
            start(gather_copy(m, p, 0))
        for q in range(pieces):
            start(token_copy(m, q))
    for m in range(2):
        start(sibling_copy(m))

    unpacked = []
    for a in FIRST:
        if a == -1:
            for m in range(2):
                transpose(m, 0)
                sibling_copy(m).wait_recv()
                transpose(m, 1)
        elif a < 0:
            forward((-2 - a) // 2, (-2 - a) % 2)
        else:
            m, p, k = a // 100, a // 10 % 10, a % 10
            gather_copy(m, p, k).wait_recv()
            if k < STEPS - 1:
                start(gather_copy(m, p, k + 1))
                continue
            unpack(m, p)
            if not unpacked:
                for q in range(pieces):
                    forward_copy(0, q).wait_recv()
                transpose(0, 2)
                transpose(0, 3)
            unpacked.append(p)
            if p ^ 1 in unpacked:
                forward_block(p // 2)

    if -4 not in FIRST:
        forward(1, 0)
    forward(1, 1)
    transpose(1, 2)
    for q in range(pieces):
        forward_copy(1, q).wait_recv()
    transpose(1, 3)

    def twin_copy(m, p):
        place = outs.at[m, rep, pl.ds(p * SIZE, SIZE)]
        return remote(place, place, rep_s.at[m * PARTS + p], rep_r.at[m * PARTS + p], twin)

    def finish(m, p):
        n = SIZE
        reduce_copy(m, p, STEPS - 1).wait_recv()
        scale = rbuf[room(m, p, STEPS - 1)].astype(f32)
        got = decode(rbuf[pl.ds(room(m, p, STEPS - 1) + 1, n)], scale)
        value = (gbuf[pl.ds(home(m, p), n)] + got) * factor
        outs[m, rep, pl.ds(p * SIZE, n)] = value
        start(twin_copy(m, p))
        return value

    def output(i, src, dst):
        copy = pltpu.make_async_copy(src, dst, out_s.at[i])
        copy.start()
        return copy

    rounds = ((near[3], near[4], far_x), (near[1], near[2], far_y), (near[0], twin, pair))

    def energy_copy(k, i):
        return remote(ebuf.at[k, 0], ebuf.at[k, 1 + i], e_s.at[k, i], e_r.at[k, i], rounds[k][i])

    def energy_begin(k):
        for i in range(3):
            start(energy_copy(k, i))

    def energy_step(k):
        for i in range(3):
            energy_copy(k, i).wait_recv()
        ebuf[k + 1, 0] = (ebuf[k, 0] + ebuf[k, 1]) + (ebuf[k, 2] + ebuf[k, 3])
        energy_begin(k + 1)

    squares = [jnp.zeros((16, 128), f32), jnp.zeros((16, 128), f32)]
    left = [PARTS, PARTS]
    outputs = []
    row_copies = []

    def arrived(m, p, k):
        if k < STEPS - 1:
            reduce_step(m, p, k)
            return
        value = finish(m, p)
        left[m] -= 1
        if m == 1:
            total = value[0] * value[0] + value[1] * value[1]
            ebuf[0, 0, p : p + 1, :] = jnp.sum(total, axis=0, keepdims=True)
            if left[m] == 0:
                energy_begin(0)
            return
        for row in range(2):
            squares[row] = squares[row] + value[row] * value[row]
        if left[m] == 0:
            for row in range(2):
                eup[0, row * 16 : row * 16 + 16] = squares[row]
            for i, device in enumerate((sibling, twin, cross)):
                row_copies.append(start(remote(eup.at[0], eup.at[1 + i], eu_s.at[i], eu_r.at[i], device)))

    def inputs_grad(i):
        part = slice(i * half_rows, (i + 1) * half_rows)
        for n in range(width // bw):
            pre[part, n * bw : (n + 1) * bw] = contract(
                gpre[part, :], wn[0, n * bw : (n + 1) * bw, :], 1, 1
            )
        start(share_copy(i))

    def share_arrived(i):
        share_copy(i).wait_recv()
        if i == 0:
            pre[0:rows] = pre[0:rows] + part_in[0]
            return
        for q in range(pieces):
            s = slice(q * chunk, (q + 1) * chunk)
            value = pre[2 * rows + q * chunk : 2 * rows + (q + 1) * chunk] + part_in[1, s]
            coded = scale_of(jnp.max(jnp.abs(value), axis=0, keepdims=True))
            pair_out[q, 0:16] = jnp.broadcast_to(coded, (16, width))
            pair_out[q, 16 : 16 + chunk] = encode(value, coded.astype(f32))
            start(pair_copy(q))

    def pair_arrived(q):
        pair_copy(q).wait_recv()
        s = slice(q * chunk, (q + 1) * chunk)
        scale = pair_in[q, 0:16].astype(f32)[0:1]
        gin[s] = (pre[s] + decode(pair_in[q, 16 : 16 + chunk], scale)).astype(bf16)
        if q == pieces - 1:
            outputs.append(output(0, gin, gin_ref))

    def energy_end():
        for i in range(3):
            energy_copy(2, i).wait_recv()
        ebuf[3, 0] = (ebuf[2, 0] + ebuf[2, 1]) * (1.0 / width)
        ebuf[3, 1] = (ebuf[2, 2] + ebuf[2, 3]) * (1.0 / width)
        outputs.append(output(2, ebuf.at[3, 0], edn_ref.at[rep]))
        outputs.append(output(3, ebuf.at[3, 1], edn_ref.at[1 - rep]))

    def twins_arrived(m):
        for p in all_parts:
            twin_copy(m, p).wait_recv()
        outputs.append(output(4 if m == 0 else 1, outs.at[m], grad_ref.at[m]))

    def run(a):
        if a < 200:
            arrived(a // 100, a // 10 % 10, a % 10)
        elif a < 1100:
            m, j = (a - 1000) // 10, a % 10
            weight_grad(m, (gpre, act)[m], j)
        elif a < 1200:
            back_block(a - 1100)
        elif a < 1300:
            inputs_grad(a - 1200)
        elif a < 1310:
            share_arrived(a - 1300)
        elif a < 1400:
            pair_arrived(a - 1310)
        elif a < 1402:
            energy_step(a - 1400)
        elif a == 1402:
            energy_end()
        else:
            twins_arrived(1)

    for a in THEN[:-3]:
        run(a)
    twins_arrived(0)
    for a in THEN[-3:]:
        run(a)
    for copy in row_copies:
        copy.wait_recv()
    outputs.append(output(5, eup, eup_ref))
    for copy in pending:
        copy.wait_send()
    for copy in outputs:
        copy.wait()


def layout(
    gin_ref, grad_ref, eup_ref, edn_ref, gin_out, gup_out, gdn_out, eup_out, edn_out,
    gin, grad, eup, edn, both, row, in_s, out_s,
):
    pairs = ((gin_ref, gin), (grad_ref.at[1], grad.at[1]), (grad_ref.at[0], grad.at[0]), (eup_ref, eup), (edn_ref, edn))
    loads = [pltpu.make_async_copy(a, b, in_s.at[i]) for i, (a, b) in enumerate(pairs)]
    for copy in loads:
        copy.start()
    stores = []

    def store(i, src, dst):
        copy = pltpu.make_async_copy(src, dst, out_s.at[i])
        copy.start()
        stores.append(copy)

    half = gup_out.shape[1] // 2
    loads[3].wait()
    total = (eup[0] + eup[1]) + (eup[2] + eup[3])
    row[...] = jnp.sum(total.T, axis=0) * (1.0 / (4 * half))
    loads[4].wait()
    store(3, row, eup_out)
    store(4, edn, edn_out)
    loads[0].wait()
    store(0, gin, gin_out)
    for m, load, out in ((1, 1, gdn_out), (0, 2, gup_out)):
        loads[load].wait()
        for r in range(2):
            for u in range(UNITS):
                block, top = divmod(u, 2)
                left = r * half + block * 128
                both[m, top * 16 : top * 16 + 16, left : left + 128] = grad[m, r, u]
        store(load, both.at[m], out)
    for copy in stores:
        copy.wait()


def body(inputs, up_proj, down_proj, out_cotangent):
    rows, width = inputs.shape
    shard, both = up_proj.shape
    hidden = both // 2
    factor = float(rows * lax.axis_size("rep") * lax.axis_size("fs") * lax.axis_size("tp")) ** (-0.5)
    f32, bf16 = jnp.float32, jnp.bfloat16
    shape = jax.ShapeDtypeStruct
    dma = pltpu.SemaphoreType.DMA
    messages = 2 * PARTS * (31 * SIZE + 5)
    anywhere = pl.BlockSpec(memory_space=pl.ANY)
    raw = pl.pallas_call(
        functools.partial(kernel, factor),
        out_shape=(
            shape((rows, width), bf16),
            shape((2, 2, UNITS, 16, 128), f32),
            shape((4, shard, 128), f32),
            shape((2, BLOCKS, 128), f32),
        ),
        in_specs=[anywhere] * 4,
        out_specs=(anywhere,) * 4,
        scratch_shapes=[
            pltpu.VMEM((2, 4 * rows, width), bf16),
            pltpu.VMEM((2, width, 4 * rows), bf16),
            pltpu.VMEM((2 * PARTS * 32, shard, 128), bf16),
            pltpu.VMEM((2, width, hidden), bf16),
            pltpu.VMEM((4 * rows, max(hidden, width)), f32),
            pltpu.VMEM((4 * rows, hidden), bf16),
            pltpu.VMEM((4 * rows, hidden), bf16),
            pltpu.VMEM((2 * 32 * UNITS, 16, 128), f32),
            pltpu.VMEM((messages, 16, 128), bf16),
            pltpu.VMEM((messages, 16, 128), bf16),
            pltpu.VMEM((2, rows, width), f32),
            pltpu.VMEM((2, 16 + rows // 2, width), bf16),
            pltpu.VMEM((2, 16 + rows // 2, width), bf16),
            pltpu.VMEM((2, 2, UNITS, 16, 128), f32),
            pltpu.VMEM((rows, width), bf16),
            pltpu.VMEM((4, 4, BLOCKS, 128), f32),
            pltpu.VMEM((4, shard, 128), f32),
            dma((2 * PARTS + 2,)),
            dma((2, 2)),
            dma((2, 2)),
            dma((2, 2)),
            dma((2, 2)),
            dma((2,)),
            dma((2,)),
            dma((2 * PARTS, STEPS)),
            dma((2 * PARTS, STEPS)),
            dma((2 * PARTS, STEPS)),
            dma((2 * PARTS, STEPS)),
            dma((2 * PARTS,)),
            dma((2 * PARTS,)),
            dma((2,)),
            dma((2,)),
            dma((2,)),
            dma((2,)),
            dma((3, 3)),
            dma((3, 3)),
            dma((3,)),
            dma((3,)),
            dma((6,)),
        ],
        compiler_params=pltpu.CompilerParams(
            collective_id=0, has_side_effects=True, vmem_limit_bytes=60 * 2**20
        ),
        name="step",
    )(inputs, out_cotangent, up_proj, down_proj.T)
    gin, gup, gdn, eup, edn = pl.pallas_call(
        layout,
        out_shape=(
            shape((rows, width), bf16),
            shape((shard, both), f32),
            shape((shard, both), f32),
            shape((shard,), f32),
            shape((2, BLOCKS, 128), f32),
        ),
        in_specs=[anywhere] * 4,
        out_specs=(anywhere,) * 5,
        scratch_shapes=[
            pltpu.VMEM((rows, width), bf16),
            pltpu.VMEM((2, 2, UNITS, 16, 128), f32),
            pltpu.VMEM((4, shard, 128), f32),
            pltpu.VMEM((2, BLOCKS, 128), f32),
            pltpu.VMEM((2, shard, both), f32),
            pltpu.VMEM((shard,), f32),
            dma((5,)),
            dma((5,)),
        ],
        name="layout",
    )(*raw)
    return gin, gup, gdn.T, eup, edn.reshape((both,))


def solution(mesh):
    return jax.shard_map(
        body,
        mesh=mesh,
        in_specs=(
            P(("rep", "fs", "tp"), None),
            P("fs", "tp"),
            P("tp", "fs"),
            P(("rep", "fs", "tp"), None),
        ),
        out_specs=(P(("rep", "fs", "tp"), None), P("fs", "tp"), P("tp", "fs"), P("fs"), P("tp")),
        check_vma=False,
    )
```

profile of v0, /device:TPU:0, one launch (start us, length us, event | category | flops | bytes accessed | tf_op | source)
XLA Modules:
  0.0 81.8 jit_solution(11185422236222849189)
XLA Ops:
  0.6 78.6 %step.1 = (bf16[256,1024]{1,0:T(8,128)(2,1)}, f32[2,2,16,16,128]{4,3,2,1,0:T(8,128)}, f32[4,32,128]{2,1,0:T(8,128)}, f32[2,8,128]{2,1,0:T(8,128)}) custom-call(bf16[256,1024]{1,0:T(8,128)(2,1)} %x_ref.1, bf16[256,1024]{1,0:T(8,128)(2,1)} %c_ref.1, bf16[32,2048]{1,0:T(8,128)(2,1)} %u_ref.1, bf16[32,2048]{1,0:T(8,128)(2,1)} %bitcast.3), custom_call_target="tpu_custom_call" | custom-call | tf_op jit(solution)/shard_map/step/pallas_call | solution.py:628
  79.3 2.3 %layout.1 = (bf16[256,1024]{1,0:T(8,128)(2,1)}, f32[32,2048]{1,0:T(8,128)}, f32[32,2048]{1,0:T(8,128)}, f32[32]{0:T(128)}, f32[2,8,128]{2,1,0:T(8,128)}) custom-call(bf16[256,1024]{1,0:T(8,128)(2,1)} %get-tuple-element.14.gin_ref, f32[2,2,16,16,128]{4,3,2,1,0:T(8,128)} %get-tuple-element.15.grad_ref, f32[4,32,128]{2,1,0:T(8,128)} %get-tuple-element.16.eup_ref, ...), custom_call_target="tpu_custom_call" | custom-call | tf_op jit(solution)/shard_map/layout/pallas_call | solution.py:684
where the time goes:
time: 82.4 us; the launch traced here: 81.8 us
  Pallas kernels  81 us (98%)
    pallas_call x1, Pallas kernels, body(): pl.pallas_call(functools.partial(kernel, factor), out_shape=(shape((rows,...  78.6 us
    pallas_call x1, Pallas kernels, body(): pl.pallas_call(layout, out_shape=(shape((rows, width), bf16), shape((shar...  2.33 us

commit v1 on v0

--- a/solution.py
+++ b/solution.py
@@ -33,23 +33,23 @@
 REDUCE = (
     (
         (4, 3, 0, 1, 2),
-        (0, 1, 2, 4, 3),
-        (2, 4, 3, 0, 1),
-        (3, 1, 2, 0, 4),
-        (4, 0, 1, 3, 2),
-        (1, 2, 0, 4, 3),
-        (3, 4, 2, 1, 0),
-        (0, 3, 1, 2, 4),
+        (0, 2, 1, 4, 3),
+        (0, 1, 4, 3, 2),
+        (2, 4, 3, 1, 0),
+        (2, 3, 0, 4, 1),
+        (1, 0, 3, 2, 4),
+        (2, 4, 1, 0, 3),
+        (4, 0, 3, 1, 2),
     ),
     (
-        (2, 1, 3, 4, 0),
-        (4, 0, 2, 1, 3),
-        (0, 4, 2, 1, 3),
-        (4, 3, 1, 0, 2),
-        (1, 4, 2, 3, 0),
-        (4, 2, 3, 0, 1),
-        (0, 3, 1, 4, 2),
-        (2, 3, 1, 0, 4),
+        (3, 4, 0, 1, 2),
+        (2, 0, 4, 1, 3),
+        (0, 2, 3, 4, 1),
+        (4, 2, 3, 1, 0),
+        (2, 3, 0, 1, 4),
+        (3, 1, 0, 4, 2),
+        (2, 4, 0, 3, 1),
+        (1, 3, 2, 4, 0),
     ),
 )
 FIRST = (
@@ -60,13 +60,13 @@
     153, 163, 4, 14, 113, 74, 64, 24, 34, 44, 54,
 )
 THEN = (
-    1010, 1011, 1012, 1013, 1100, 1000, 1101, 100, 110, 1001, 130, 150, 1102, 140, 120, 170,
-    1002, 160, 101, 111, 1103, 10, 131, 1003, 0, 141, 151, 30, 20, 1201, 171, 161,
-    121, 132, 40, 50, 11, 112, 1200, 102, 142, 1, 152, 60, 1301, 133, 172, 122,
-    70, 162, 12, 31, 41, 51, 103, 1300, 153, 143, 21, 113, 134, 173, 123, 61,
-    163, 2, 13, 71, 42, 154, 144, 52, 32, 114, 104, 22, 174, 124, 164, 3,
-    14, 62, 43, 72, 53, 33, 23, 4, 1400, 63, 44, 1500, 54, 73, 34, 24,
-    64, 1401, 74, 1402, 1310, 1311,
+    1010, 1011, 1012, 1013, 1100, 1101, 1102, 100, 110, 1103, 120, 130, 1000, 140, 150, 1001,
+    160, 170, 1201, 101, 121, 1002, 111, 151, 1003, 0, 10, 131, 171, 1301, 30, 161,
+    141, 102, 122, 1200, 20, 152, 50, 40, 112, 162, 60, 70, 1, 142, 132, 172,
+    11, 1300, 123, 103, 31, 21, 153, 113, 51, 41, 143, 163, 133, 173, 61, 104,
+    71, 2, 12, 124, 114, 32, 154, 22, 144, 134, 52, 164, 42, 174, 62, 72,
+    13, 3, 33, 23, 53, 43, 1400, 63, 73, 4, 1500, 14, 34, 24, 54, 44,
+    64, 74, 1401, 1402, 1310, 1311,
 )
 STEPS = 5
 PARTS = 8
@@ -145,31 +145,24 @@
     part_in,
     pair_out,
     pair_in,
+    twin_out,
+    twin_in,
     outs,
     gin,
     ebuf,
     eup,
     load_s,
-    tok_s,
     tok_r,
-    fwd_s,
     fwd_r,
-    sib_s,
     sib_r,
-    g_s,
     g_r,
-    r_s,
     r_r,
-    rep_s,
     rep_r,
-    pi_s,
     pi_r,
-    li_s,
     li_r,
-    e_s,
     e_r,
-    eu_s,
     eu_r,
+    sent,
     out_s,
 ):
     rep, fs, tp = lax.axis_index("rep"), lax.axis_index("fs"), lax.axis_index("tp")
@@ -223,35 +216,30 @@
     for device in near + [sibling, pair, twin, cross, far_x, far_y]:
         pl.semaphore_signal(barrier, inc=1, device_id=device, device_id_type=MESH)
 
-    loads = []
     for m in range(2):
-        loads.append(pltpu.make_async_copy(tokens[m], tok.at[m, pl.ds(0, rows)], load_s.at[16 + m]))
+        pltpu.make_async_copy(tokens[m], tok.at[m, pl.ds(0, rows)], load_s.at[m]).start()
         for p in all_parts:
             columns = pl.ds(pl.multiple_of(base + p * 128, 128), 128)
-            loads.append(
-                pltpu.make_async_copy(
-                    weights[m].at[:, columns], wg.at[place_of(m, p)], load_s.at[m * PARTS + p]
-                )
-            )
-    for copy in loads:
-        copy.start()
-    for copy in loads:
-        copy.wait()
+            pltpu.make_async_copy(weights[m].at[:, columns], wg.at[place_of(m, p)], load_s.at[2 + m]).start()
+
+    def wait_bytes(ref, sem):
+        pltpu.make_async_copy(ref, ref, sem).wait()
+
+    for m in range(2):
+        wait_bytes(tok.at[m, pl.ds(0, rows)], load_s.at[m])
+        wait_bytes(wg.at[pl.ds(0, PARTS)], load_s.at[2 + m])
 
     pl.semaphore_wait(barrier, STEPS + 6)
-
-    pending = []
 
     def start(copy):
         copy.start()
-        pending.append(copy)
         return copy
 
     def token_copy(m, q):
         return remote(
             tok.at[m, pl.ds(q * chunk, chunk)],
             tok.at[m, pl.ds(2 * rows + q * chunk, chunk)],
-            tok_s.at[m, q],
+            sent.at[0],
             tok_r.at[m, q],
             pair,
         )
@@ -260,20 +248,20 @@
         return remote(
             tok.at[m, pl.ds(2 * rows + q * chunk, chunk)],
             tok.at[m, pl.ds(3 * rows + q * chunk, chunk)],
-            fwd_s.at[m, q],
+            sent.at[1],
             fwd_r.at[m, q],
             sibling,
         )
 
     def sibling_copy(m):
-        return remote(tok.at[m, pl.ds(0, rows)], tok.at[m, pl.ds(rows, rows)], sib_s.at[m], sib_r.at[m], sibling)
+        return remote(tok.at[m, pl.ds(0, rows)], tok.at[m, pl.ds(rows, rows)], sent.at[2], sib_r.at[m], sibling)
 
     def gather_copy(m, p, k):
         n = 2**k
         return remote(
             wg.at[pl.ds(place_of(m, p), n)],
             wg.at[pl.ds(place_of(m, p) + n, n)],
-            g_s.at[m * PARTS + p, k],
+            sent.at[3 + m],
             g_r.at[m * PARTS + p, k],
             near[GATHER[m][p][k]],
         )
@@ -321,7 +309,7 @@
         return remote(
             sbuf.at[place],
             rbuf.at[place],
-            r_s.at[m * PARTS + p, k],
+            sent.at[5],
             r_r.at[m * PARTS + p, k],
             near[REDUCE[m][p][STEPS - 1 - k]],
         )
@@ -396,11 +384,11 @@
 
     def share_copy(i):
         return remote(
-            pre.at[pl.ds((1 + 2 * i) * rows, rows)], part_in.at[i], pi_s.at[i], pi_r.at[i], sibling
+            pre.at[pl.ds((1 + 2 * i) * rows, rows)], part_in.at[i], sent.at[6], pi_r.at[i], sibling
         )
 
     def pair_copy(q):
-        return remote(pair_out.at[q], pair_in.at[q], li_s.at[q], li_r.at[q], pair)
+        return remote(pair_out.at[q], pair_in.at[q], sent.at[7], li_r.at[q], pair)
 
     for m in range(2):
         for p in all_parts:
@@ -443,9 +431,38 @@
         forward_copy(1, q).wait_recv()
     transpose(1, 3)
 
-    def twin_copy(m, p):
-        place = outs.at[m, rep, pl.ds(p * SIZE, SIZE)]
-        return remote(place, place, rep_s.at[m * PARTS + p], rep_r.at[m * PARTS + p], twin)
+    order = [a // 10 % 10 for a in THEN if a < 100 and a % 10 == STEPS - 1]
+    groups = (tuple(all_parts), tuple(order[:4]), tuple(order[4:]))
+    spots = (0, 17, 26)
+
+    def twin_copy(g):
+        place = pl.ds(spots[g], 1 + len(groups[g]) * SIZE)
+        return remote(twin_out.at[place], twin_in.at[place], sent.at[10], rep_r.at[g], twin)
+
+    def twin_send(g):
+        m = 1 if g == 0 else 0
+        top = jnp.zeros((16, 128), f32)
+        for p in groups[g]:
+            for i in range(SIZE):
+                top = jnp.maximum(top, jnp.abs(outs[m, rep, p * SIZE + i]))
+        coded = scale_of(top)
+        twin_out[spots[g]] = coded
+        scale = coded.astype(f32)
+        for n, p in enumerate(groups[g]):
+            code = encode(outs[m, rep, pl.ds(p * SIZE, SIZE)], scale)
+            twin_out[pl.ds(spots[g] + 1 + n * SIZE, SIZE)] = code
+        start(twin_copy(g))
+        for n, p in enumerate(groups[g]):
+            code = twin_out[pl.ds(spots[g] + 1 + n * SIZE, SIZE)]
+            outs[m, rep, pl.ds(p * SIZE, SIZE)] = decode(code, scale)
+
+    def twin_receive(g):
+        m = 1 if g == 0 else 0
+        twin_copy(g).wait_recv()
+        scale = twin_in[spots[g]].astype(f32)
+        for n, p in enumerate(groups[g]):
+            code = twin_in[pl.ds(spots[g] + 1 + n * SIZE, SIZE)]
+            outs[m, 1 - rep, pl.ds(p * SIZE, SIZE)] = decode(code, scale)
 
     def finish(m, p):
         n = SIZE
@@ -454,7 +471,6 @@
         got = decode(rbuf[pl.ds(room(m, p, STEPS - 1) + 1, n)], scale)
         value = (gbuf[pl.ds(home(m, p), n)] + got) * factor
         outs[m, rep, pl.ds(p * SIZE, n)] = value
-        start(twin_copy(m, p))
         return value
 
     def output(i, src, dst):
@@ -465,7 +481,7 @@
     rounds = ((near[3], near[4], far_x), (near[1], near[2], far_y), (near[0], twin, pair))
 
     def energy_copy(k, i):
-        return remote(ebuf.at[k, 0], ebuf.at[k, 1 + i], e_s.at[k, i], e_r.at[k, i], rounds[k][i])
+        return remote(ebuf.at[k, 0], ebuf.at[k, 1 + i], sent.at[8], e_r.at[k, i], rounds[k][i])
 
     def energy_begin(k):
         for i in range(3):
@@ -493,14 +509,18 @@
             ebuf[0, 0, p : p + 1, :] = jnp.sum(total, axis=0, keepdims=True)
             if left[m] == 0:
                 energy_begin(0)
+                twin_send(0)
             return
         for row in range(2):
             squares[row] = squares[row] + value[row] * value[row]
+        if left[m] == 4:
+            twin_send(1)
         if left[m] == 0:
+            twin_send(2)
             for row in range(2):
                 eup[0, row * 16 : row * 16 + 16] = squares[row]
             for i, device in enumerate((sibling, twin, cross)):
-                row_copies.append(start(remote(eup.at[0], eup.at[1 + i], eu_s.at[i], eu_r.at[i], device)))
+                row_copies.append(start(remote(eup.at[0], eup.at[1 + i], sent.at[9], eu_r.at[i], device)))
 
     def inputs_grad(i):
         part = slice(i * half_rows, (i + 1) * half_rows)
@@ -540,8 +560,8 @@
         outputs.append(output(3, ebuf.at[3, 1], edn_ref.at[1 - rep]))
 
     def twins_arrived(m):
-        for p in all_parts:
-            twin_copy(m, p).wait_recv()
+        for g in (0,) if m == 1 else (1, 2):
+            twin_receive(g)
         outputs.append(output(4 if m == 0 else 1, outs.at[m], grad_ref.at[m]))
 
     def run(a):
@@ -573,8 +593,17 @@
     for copy in row_copies:
         copy.wait_recv()
     outputs.append(output(5, eup, eup_ref))
-    for copy in pending:
-        copy.wait_send()
+    wait_bytes(tok.at[:, pl.ds(0, rows)], sent.at[0])
+    wait_bytes(tok.at[:, pl.ds(0, rows)], sent.at[1])
+    wait_bytes(tok.at[:, pl.ds(0, rows)], sent.at[2])
+    for m in range(2):
+        wait_bytes(wg.at[pl.ds(0, 31 * PARTS)], sent.at[3 + m])
+    wait_bytes(sbuf, sent.at[5])
+    wait_bytes(part_in, sent.at[6])
+    wait_bytes(pair_out, sent.at[7])
+    wait_bytes(ebuf.at[pl.ds(0, 3), pl.ds(0, 3)], sent.at[8])
+    wait_bytes(eup.at[pl.ds(0, 3)], sent.at[9])
+    wait_bytes(twin_out, sent.at[10])
     for copy in outputs:
         copy.wait()
 
@@ -649,31 +678,24 @@
             pltpu.VMEM((2, rows, width), f32),
             pltpu.VMEM((2, 16 + rows // 2, width), bf16),
             pltpu.VMEM((2, 16 + rows // 2, width), bf16),
+            pltpu.VMEM((35, 16, 128), bf16),
+            pltpu.VMEM((35, 16, 128), bf16),
             pltpu.VMEM((2, 2, UNITS, 16, 128), f32),
             pltpu.VMEM((rows, width), bf16),
             pltpu.VMEM((4, 4, BLOCKS, 128), f32),
             pltpu.VMEM((4, shard, 128), f32),
-            dma((2 * PARTS + 2,)),
-            dma((2, 2)),
-            dma((2, 2)),
+            dma((4,)),
             dma((2, 2)),
             dma((2, 2)),
             dma((2,)),
-            dma((2,)),
             dma((2 * PARTS, STEPS)),
             dma((2 * PARTS, STEPS)),
-            dma((2 * PARTS, STEPS)),
-            dma((2 * PARTS, STEPS)),
-            dma((2 * PARTS,)),
-            dma((2 * PARTS,)),
-            dma((2,)),
-            dma((2,)),
+            dma((3,)),
             dma((2,)),
             dma((2,)),
             dma((3, 3)),
-            dma((3, 3)),
             dma((3,)),
-            dma((3,)),
+            dma((11,)),
             dma((6,)),
         ],
         compiler_params=pltpu.CompilerParams(

time: 82.4 us -> 79.1 us (0.960)
  Pallas kernels: 81 us -> 77.9 us
    pallas_call x1, Pallas kernels: 78.6 us -> 75.6 us  [body(): pl.pallas_call(functools.partial(kernel, factor), out_shape=(shape((rows,...]
where the time goes in v1:
time: 79.1 us; the launch traced here: 78.7 us
  Pallas kernels  77.9 us (98%)
  between operations  0.82 us (1%)
    pallas_call x1, Pallas kernels, body(): pl.pallas_call(functools.partial(kernel, factor), out_shape=(shape((rows,...  75.6 us
    pallas_call x1, Pallas kernels, body(): pl.pallas_call(layout, out_shape=(shape((rows, width), bf16), shape((shar...  2.33 us

profile of v1, /device:TPU:0, one launch (start us, length us, event | category | flops | bytes accessed | tf_op | source)
XLA Modules:
  0.0 78.7 jit_solution(17447585326280556020)
XLA Ops:
  0.6 75.6 %step.1 = (bf16[256,1024]{1,0:T(8,128)(2,1)}, f32[2,2,16,16,128]{4,3,2,1,0:T(8,128)}, f32[4,32,128]{2,1,0:T(8,128)}, f32[2,8,128]{2,1,0:T(8,128)}) custom-call(bf16[256,1024]{1,0:T(8,128)(2,1)} %x_ref.1, bf16[256,1024]{1,0:T(8,128)(2,1)} %c_ref.1, bf16[32,2048]{1,0:T(8,128)(2,1)} %u_ref.1, bf16[32,2048]{1,0:T(8,128)(2,1)} %bitcast.3), custom_call_target="tpu_custom_call" | custom-call | tf_op jit(solution)/shard_map/step/pallas_call | solution.py:657
  76.2 2.3 %layout.1 = (bf16[256,1024]{1,0:T(8,128)(2,1)}, f32[32,2048]{1,0:T(8,128)}, f32[32,2048]{1,0:T(8,128)}, f32[32]{0:T(128)}, f32[2,8,128]{2,1,0:T(8,128)}) custom-call(bf16[256,1024]{1,0:T(8,128)(2,1)} %get-tuple-element.14.gin_ref, f32[2,2,16,16,128]{4,3,2,1,0:T(8,128)} %get-tuple-element.15.grad_ref, f32[4,32,128]{2,1,0:T(8,128)} %get-tuple-element.16.eup_ref, ...), custom_call_target="tpu_custom_call" | custom-call | tf_op jit(solution)/shard_map/layout/pallas_call | solution.py:706

commit v2 on v1

--- a/solution.py
+++ b/solution.py
@@ -61,9 +61,9 @@
 )
 THEN = (
     1010, 1011, 1012, 1013, 1100, 1101, 1102, 100, 110, 1103, 120, 130, 1000, 140, 150, 1001,
-    160, 170, 1201, 101, 121, 1002, 111, 151, 1003, 0, 10, 131, 171, 1301, 30, 161,
-    141, 102, 122, 1200, 20, 152, 50, 40, 112, 162, 60, 70, 1, 142, 132, 172,
-    11, 1300, 123, 103, 31, 21, 153, 113, 51, 41, 143, 163, 133, 173, 61, 104,
+    160, 170, 101, 121, 1002, 111, 151, 1003, 1201, 0, 10, 131, 171, 1200, 30, 161,
+    141, 1301, 102, 122, 20, 152, 1300, 50, 40, 112, 162, 60, 70, 1, 142, 132,
+    172, 11, 123, 103, 31, 21, 153, 113, 51, 41, 143, 163, 133, 173, 61, 104,
     71, 2, 12, 124, 114, 32, 154, 22, 144, 134, 52, 164, 42, 174, 62, 72,
     13, 3, 33, 23, 53, 43, 1400, 63, 73, 4, 1500, 14, 34, 24, 54, 44,
     64, 74, 1401, 1402, 1310, 1311,
@@ -183,6 +183,7 @@
     tokens = (x_ref, c_ref)
     pieces = 2
     chunk = rows // pieces
+    cuts = (2, 4)
     half_rows = 2 * rows
     bw = 256
     blocks = hidden // bw
@@ -237,8 +238,8 @@
 
     def token_copy(m, q):
         return remote(
-            tok.at[m, pl.ds(q * chunk, chunk)],
-            tok.at[m, pl.ds(2 * rows + q * chunk, chunk)],
+            tok.at[m, pl.ds(q * (rows // cuts[m]), rows // cuts[m])],
+            tok.at[m, pl.ds(2 * rows + q * (rows // cuts[m]), rows // cuts[m])],
             sent.at[0],
             tok_r.at[m, q],
             pair,
@@ -246,8 +247,8 @@
 
     def forward_copy(m, q):
         return remote(
-            tok.at[m, pl.ds(2 * rows + q * chunk, chunk)],
-            tok.at[m, pl.ds(3 * rows + q * chunk, chunk)],
+            tok.at[m, pl.ds(2 * rows + q * (rows // cuts[m]), rows // cuts[m])],
+            tok.at[m, pl.ds(3 * rows + q * (rows // cuts[m]), rows // cuts[m])],
             sent.at[1],
             fwd_r.at[m, q],
             sibling,
@@ -393,7 +394,7 @@
     for m in range(2):
         for p in all_parts:
             start(gather_copy(m, p, 0))
-        for q in range(pieces):
+        for q in range(cuts[m]):
             start(token_copy(m, q))
     for m in range(2):
         start(sibling_copy(m))
@@ -423,17 +424,16 @@
             if p ^ 1 in unpacked:
                 forward_block(p // 2)
 
-    if -4 not in FIRST:
-        forward(1, 0)
-    forward(1, 1)
+    for q in range(cuts[1]):
+        forward(1, q)
     transpose(1, 2)
-    for q in range(pieces):
+    for q in range(cuts[1]):
         forward_copy(1, q).wait_recv()
     transpose(1, 3)
 
     order = [a // 10 % 10 for a in THEN if a < 100 and a % 10 == STEPS - 1]
-    groups = (tuple(all_parts), tuple(order[:4]), tuple(order[4:]))
-    spots = (0, 17, 26)
+    groups = (tuple(all_parts), tuple(order[:6]), tuple(order[6:]))
+    spots = (0, 17, 30)
 
     def twin_copy(g):
         place = pl.ds(spots[g], 1 + len(groups[g]) * SIZE)
@@ -513,7 +513,7 @@
             return
         for row in range(2):
             squares[row] = squares[row] + value[row] * value[row]
-        if left[m] == 4:
+        if left[m] == 2:
             twin_send(1)
         if left[m] == 0:
             twin_send(2)
@@ -685,8 +685,8 @@
             pltpu.VMEM((4, 4, BLOCKS, 128), f32),
             pltpu.VMEM((4, shard, 128), f32),
             dma((4,)),
-            dma((2, 2)),
-            dma((2, 2)),
+            dma((2, 4)),
+            dma((2, 4)),
             dma((2,)),
             dma((2 * PARTS, STEPS)),
             dma((2 * PARTS, STEPS)),

time: 79.1 us -> 79.3 us (level)
  no operation moved by 1% of the time
where the time goes in v2:
time: 79.3 us; the launch traced here: 79 us
  Pallas kernels  78.2 us (99%)
  between operations  0.82 us (1%)
    pallas_call x1, Pallas kernels, body(): pl.pallas_call(functools.partial(kernel, factor), out_shape=(shape((rows,...  75.8 us
    pallas_call x1, Pallas kernels, body(): pl.pallas_call(layout, out_shape=(shape((rows, width), bf16), shape((shar...  2.33 us

profile of v2, /device:TPU:0, one launch (start us, length us, event | category | flops | bytes accessed | tf_op | source)
XLA Modules:
  0.0 79.0 jit_solution(4496547275541503027)
XLA Ops:
  0.6 75.8 %step.1 = (bf16[256,1024]{1,0:T(8,128)(2,1)}, f32[2,2,16,16,128]{4,3,2,1,0:T(8,128)}, f32[4,32,128]{2,1,0:T(8,128)}, f32[2,8,128]{2,1,0:T(8,128)}) custom-call(bf16[256,1024]{1,0:T(8,128)(2,1)} %x_ref.1, bf16[256,1024]{1,0:T(8,128)(2,1)} %c_ref.1, bf16[32,2048]{1,0:T(8,128)(2,1)} %u_ref.1, bf16[32,2048]{1,0:T(8,128)(2,1)} %bitcast.3), custom_call_target="tpu_custom_call" | custom-call | tf_op jit(solution)/shard_map/step/pallas_call | solution.py:657
  76.5 2.3 %layout.1 = (bf16[256,1024]{1,0:T(8,128)(2,1)}, f32[32,2048]{1,0:T(8,128)}, f32[32,2048]{1,0:T(8,128)}, f32[32]{0:T(128)}, f32[2,8,128]{2,1,0:T(8,128)}) custom-call(bf16[256,1024]{1,0:T(8,128)(2,1)} %get-tuple-element.14.gin_ref, f32[2,2,16,16,128]{4,3,2,1,0:T(8,128)} %get-tuple-element.15.grad_ref, f32[4,32,128]{2,1,0:T(8,128)} %get-tuple-element.16.eup_ref, ...), custom_call_target="tpu_custom_call" | custom-call | tf_op jit(solution)/shard_map/layout/pallas_call | solution.py:706

commit v3 on v2

--- a/solution.py
+++ b/solution.py
@@ -32,24 +32,24 @@
 )
 REDUCE = (
     (
+        (3, 4, 2, 0, 1),
         (4, 3, 0, 1, 2),
-        (0, 2, 1, 4, 3),
-        (0, 1, 4, 3, 2),
-        (2, 4, 3, 1, 0),
-        (2, 3, 0, 4, 1),
-        (1, 0, 3, 2, 4),
-        (2, 4, 1, 0, 3),
-        (4, 0, 3, 1, 2),
+        (1, 2, 0, 4, 3),
+        (2, 1, 0, 4, 3),
+        (3, 4, 0, 2, 1),
+        (3, 4, 2, 1, 0),
+        (2, 1, 0, 3, 4),
+        (3, 4, 1, 0, 2),
     ),
     (
-        (3, 4, 0, 1, 2),
-        (2, 0, 4, 1, 3),
-        (0, 2, 3, 4, 1),
-        (4, 2, 3, 1, 0),
-        (2, 3, 0, 1, 4),
-        (3, 1, 0, 4, 2),
-        (2, 4, 0, 3, 1),
-        (1, 3, 2, 4, 0),
+        (1, 2, 0, 4, 3),
+        (4, 3, 1, 0, 2),
+        (1, 2, 4, 3, 0),
+        (4, 3, 2, 0, 1),
+        (2, 1, 0, 4, 3),
+        (4, 3, 0, 2, 1),
+        (1, 2, 3, 0, 4),
+        (2, 1, 3, 4, 0),
     ),
 )
 FIRST = (
@@ -60,13 +60,12 @@
     153, 163, 4, 14, 113, 74, 64, 24, 34, 44, 54,
 )
 THEN = (
-    1010, 1011, 1012, 1013, 1100, 1101, 1102, 100, 110, 1103, 120, 130, 1000, 140, 150, 1001,
-    160, 170, 101, 121, 1002, 111, 151, 1003, 1201, 0, 10, 131, 171, 1200, 30, 161,
-    141, 1301, 102, 122, 20, 152, 1300, 50, 40, 112, 162, 60, 70, 1, 142, 132,
-    172, 11, 123, 103, 31, 21, 153, 113, 51, 41, 143, 163, 133, 173, 61, 104,
-    71, 2, 12, 124, 114, 32, 154, 22, 144, 134, 52, 164, 42, 174, 62, 72,
-    13, 3, 33, 23, 53, 43, 1400, 63, 73, 4, 1500, 14, 34, 24, 54, 44,
-    64, 74, 1401, 1402, 1310, 1311,
+    1010, 1011, 1012, 1013, 1100, 1101, 1102, 100, 110, 1103, 120, 130, 1000, 140, 160, 1001,
+    170, 150, 101, 1002, 111, 121, 1003, 131, 141, 1201, 0, 161, 10, 171, 102, 1200,
+    122, 20, 151, 40, 1301, 50, 112, 60, 30, 70, 142, 162, 1300, 132, 11, 172,
+    1, 103, 152, 21, 123, 41, 51, 113, 31, 61, 71, 143, 163, 12, 133, 173,
+    2, 22, 153, 42, 52, 32, 72, 62, 13, 3, 1400, 23, 43, 1500, 53, 33,
+    73, 63, 1401, 1402, 1310, 1311,
 )
 STEPS = 5
 PARTS = 8
@@ -74,7 +73,9 @@
 SIZE = 2
 UNITS = 16
 BLOCKS = 8
-HALF = (16, 8, 4, 2, 1)
+HALF = (16, 8, 4)
+HALVINGS = 3
+ROOM = 68
 SPAN = 240.0
 SHIFT = 120.0
 
@@ -303,7 +304,7 @@
 
     def room(m, p, k):
         before = sum(1 + HALF[i] * SIZE for i in range(k))
-        return (m * PARTS + p) * (31 * SIZE + 5) + before
+        return (m * PARTS + p) * ROOM + before
 
     def reduce_copy(m, p, k):
         place = pl.ds(room(m, p, k), 1 + HALF[k] * SIZE)
@@ -315,6 +316,21 @@
             near[REDUCE[m][p][STEPS - 1 - k]],
         )
 
+    def direct_room(m, p, i):
+        return room(m, p, HALVINGS) + (i - 1) * (1 + SIZE)
+
+    def direct_copy(m, p, i):
+        order = REDUCE[m][p]
+        far = far_x if 3 in order[:2] else far_y
+        place = pl.ds(direct_room(m, p, i), 1 + SIZE)
+        return remote(
+            sbuf.at[place],
+            rbuf.at[place],
+            sent.at[5],
+            r_r.at[m * PARTS + p, HALVINGS + i - 1],
+            (None, near[order[0]], near[order[1]], far)[i],
+        )
+
     def chunks(count, size):
         step = min(count, 4) * size
         return count * size // step, step
@@ -363,6 +379,21 @@
 
     def reduce_step(m, p, k):
         reduce_copy(m, p, k).wait_recv()
+        if k == HALVINGS - 1:
+            scale = rbuf[room(m, p, k)].astype(f32)
+            for i in (3, 2, 1, 0):
+                at = home(m, p) + i * SIZE
+                got = room(m, p, k) + 1 + i * SIZE
+                value = gbuf[pl.ds(at, SIZE)] + decode(rbuf[pl.ds(got, SIZE)], scale)
+                if i == 0:
+                    gbuf[pl.ds(at, SIZE)] = value
+                    continue
+                coded = scale_of(jnp.max(jnp.abs(value), axis=0))
+                to = direct_room(m, p, i)
+                sbuf[to] = coded
+                sbuf[pl.ds(to + 1, SIZE)] = encode(value, coded.astype(f32))
+                start(direct_copy(m, p, i))
+            return
         n = HALF[k + 1]
         top = add_sums(m, p, k, n, n)
         send_sums(m, p, k + 1, top)
@@ -431,7 +462,7 @@
         forward_copy(1, q).wait_recv()
     transpose(1, 3)
 
-    order = [a // 10 % 10 for a in THEN if a < 100 and a % 10 == STEPS - 1]
+    order = [a // 10 % 10 for a in THEN if a < 100 and a % 10 == HALVINGS]
     groups = (tuple(all_parts), tuple(order[:6]), tuple(order[6:]))
     spots = (0, 17, 30)
 
@@ -465,12 +496,13 @@
             outs[m, 1 - rep, pl.ds(p * SIZE, SIZE)] = decode(code, scale)
 
     def finish(m, p):
-        n = SIZE
-        reduce_copy(m, p, STEPS - 1).wait_recv()
-        scale = rbuf[room(m, p, STEPS - 1)].astype(f32)
-        got = decode(rbuf[pl.ds(room(m, p, STEPS - 1) + 1, n)], scale)
-        value = (gbuf[pl.ds(home(m, p), n)] + got) * factor
-        outs[m, rep, pl.ds(p * SIZE, n)] = value
+        value = gbuf[pl.ds(home(m, p), SIZE)]
+        for i in (1, 2, 3):
+            direct_copy(m, p, i).wait_recv()
+            to = direct_room(m, p, i)
+            value = value + decode(rbuf[pl.ds(to + 1, SIZE)], rbuf[to].astype(f32))
+        value = value * factor
+        outs[m, rep, pl.ds(p * SIZE, SIZE)] = value
         return value
 
     def output(i, src, dst):
@@ -499,7 +531,7 @@
     row_copies = []
 
     def arrived(m, p, k):
-        if k < STEPS - 1:
+        if k < HALVINGS:
             reduce_step(m, p, k)
             return
         value = finish(m, p)
@@ -652,7 +684,7 @@
     f32, bf16 = jnp.float32, jnp.bfloat16
     shape = jax.ShapeDtypeStruct
     dma = pltpu.SemaphoreType.DMA
-    messages = 2 * PARTS * (31 * SIZE + 5)
+    messages = 2 * PARTS * ROOM
     anywhere = pl.BlockSpec(memory_space=pl.ANY)
     raw = pl.pallas_call(
         functools.partial(kernel, factor),
@@ -689,7 +721,7 @@
             dma((2, 4)),
             dma((2,)),
             dma((2 * PARTS, STEPS)),
-            dma((2 * PARTS, STEPS)),
+            dma((2 * PARTS, 6)),
             dma((3,)),
             dma((2,)),
             dma((2,)),

time: 79.3 us -> 76.3 us (0.962)
  Pallas kernels: 78.2 us -> 74.8 us
    pallas_call x1, Pallas kernels: 75.8 us -> 72.5 us  [body(): pl.pallas_call(functools.partial(kernel, factor), out_shape=(shape((rows,...]
where the time goes in v3:
time: 76.3 us; the launch traced here: 75.6 us
  Pallas kernels  74.8 us (98%)
  between operations  0.82 us (1%)
    pallas_call x1, Pallas kernels, body(): pl.pallas_call(functools.partial(kernel, factor), out_shape=(shape((rows,...  72.5 us
    pallas_call x1, Pallas kernels, body(): pl.pallas_call(layout, out_shape=(shape((rows, width), bf16), shape((shar...  2.33 us

profile of v3, /device:TPU:0, one launch (start us, length us, event | category | flops | bytes accessed | tf_op | source)
XLA Modules:
  0.0 75.6 jit_solution(12953450004479214372)
XLA Ops:
  0.6 72.5 %step.1 = (bf16[256,1024]{1,0:T(8,128)(2,1)}, f32[2,2,16,16,128]{4,3,2,1,0:T(8,128)}, f32[4,32,128]{2,1,0:T(8,128)}, f32[2,8,128]{2,1,0:T(8,128)}) custom-call(bf16[256,1024]{1,0:T(8,128)(2,1)} %x_ref.1, bf16[256,1024]{1,0:T(8,128)(2,1)} %c_ref.1, bf16[32,2048]{1,0:T(8,128)(2,1)} %u_ref.1, bf16[32,2048]{1,0:T(8,128)(2,1)} %bitcast.3), custom_call_target="tpu_custom_call" | custom-call | tf_op jit(solution)/shard_map/step/pallas_call | solution.py:689
  73.1 2.3 %layout.1 = (bf16[256,1024]{1,0:T(8,128)(2,1)}, f32[32,2048]{1,0:T(8,128)}, f32[32,2048]{1,0:T(8,128)}, f32[32]{0:T(128)}, f32[2,8,128]{2,1,0:T(8,128)}) custom-call(bf16[256,1024]{1,0:T(8,128)(2,1)} %get-tuple-element.14.gin_ref, f32[2,2,16,16,128]{4,3,2,1,0:T(8,128)} %get-tuple-element.15.grad_ref, f32[4,32,128]{2,1,0:T(8,128)} %get-tuple-element.16.eup_ref, ...), custom_call_target="tpu_custom_call" | custom-call | tf_op jit(solution)/shard_map/layout/pallas_call | solution.py:738

commit v4 on v3

--- a/solution.py
+++ b/solution.py
@@ -327,12 +327,12 @@
             sbuf.at[place],
             rbuf.at[place],
             sent.at[5],
-            r_r.at[m * PARTS + p, HALVINGS + i - 1],
+            r_r.at[m * PARTS + p, HALVINGS],
             (None, near[order[0]], near[order[1]], far)[i],
         )
 
     def chunks(count, size):
-        step = min(count, 4) * size
+        step = min(count, 8) * size
         return count * size // step, step
 
     def highest(m, p, k):
@@ -497,8 +497,8 @@
 
     def finish(m, p):
         value = gbuf[pl.ds(home(m, p), SIZE)]
+        wait_bytes(rbuf.at[pl.ds(direct_room(m, p, 1), 3 * (1 + SIZE))], r_r.at[m * PARTS + p, HALVINGS])
         for i in (1, 2, 3):
-            direct_copy(m, p, i).wait_recv()
             to = direct_room(m, p, i)
             value = value + decode(rbuf[pl.ds(to + 1, SIZE)], rbuf[to].astype(f32))
         value = value * factor
@@ -513,15 +513,14 @@
     rounds = ((near[3], near[4], far_x), (near[1], near[2], far_y), (near[0], twin, pair))
 
     def energy_copy(k, i):
-        return remote(ebuf.at[k, 0], ebuf.at[k, 1 + i], sent.at[8], e_r.at[k, i], rounds[k][i])
+        return remote(ebuf.at[k, 0], ebuf.at[k, 1 + i], sent.at[8], e_r.at[k], rounds[k][i])
 
     def energy_begin(k):
         for i in range(3):
             start(energy_copy(k, i))
 
     def energy_step(k):
-        for i in range(3):
-            energy_copy(k, i).wait_recv()
+        wait_bytes(ebuf.at[k, pl.ds(1, 3)], e_r.at[k])
         ebuf[k + 1, 0] = (ebuf[k, 0] + ebuf[k, 1]) + (ebuf[k, 2] + ebuf[k, 3])
         energy_begin(k + 1)
 
@@ -552,7 +551,7 @@
             for row in range(2):
                 eup[0, row * 16 : row * 16 + 16] = squares[row]
             for i, device in enumerate((sibling, twin, cross)):
-                row_copies.append(start(remote(eup.at[0], eup.at[1 + i], sent.at[9], eu_r.at[i], device)))
+                row_copies.append(start(remote(eup.at[0], eup.at[1 + i], sent.at[9], eu_r.at[0], device)))
 
     def inputs_grad(i):
         part = slice(i * half_rows, (i + 1) * half_rows)
@@ -584,8 +583,7 @@
             outputs.append(output(0, gin, gin_ref))
 
     def energy_end():
-        for i in range(3):
-            energy_copy(2, i).wait_recv()
+        wait_bytes(ebuf.at[2, pl.ds(1, 3)], e_r.at[2])
         ebuf[3, 0] = (ebuf[2, 0] + ebuf[2, 1]) * (1.0 / width)
         ebuf[3, 1] = (ebuf[2, 2] + ebuf[2, 3]) * (1.0 / width)
         outputs.append(output(2, ebuf.at[3, 0], edn_ref.at[rep]))
@@ -622,8 +620,7 @@
     twins_arrived(0)
     for a in THEN[-3:]:
         run(a)
-    for copy in row_copies:
-        copy.wait_recv()
+    wait_bytes(eup.at[pl.ds(1, 3)], eu_r.at[0])
     outputs.append(output(5, eup, eup_ref))
     wait_bytes(tok.at[:, pl.ds(0, rows)], sent.at[0])
     wait_bytes(tok.at[:, pl.ds(0, rows)], sent.at[1])
@@ -721,12 +718,12 @@
             dma((2, 4)),
             dma((2,)),
             dma((2 * PARTS, STEPS)),
-            dma((2 * PARTS, 6)),
+            dma((2 * PARTS, HALVINGS + 1)),
             dma((3,)),
             dma((2,)),
             dma((2,)),
-            dma((3, 3)),
             dma((3,)),
+            dma((1,)),
             dma((11,)),
             dma((6,)),
         ],

time: 76.3 us -> 75.7 us (level)
  no operation moved by 1% of the time
where the time goes in v4:
time: 75.7 us; the launch traced here: 75 us
  Pallas kernels  74.2 us (98%)
  between operations  0.82 us (1%)
    pallas_call x1, Pallas kernels, body(): pl.pallas_call(functools.partial(kernel, factor), out_shape=(shape((rows,...  71.8 us
    pallas_call x1, Pallas kernels, body(): pl.pallas_call(layout, out_shape=(shape((rows, width), bf16), shape((shar...  2.33 us

profile of v4, /device:TPU:0, one launch (start us, length us, event | category | flops | bytes accessed | tf_op | source)
XLA Modules:
  0.0 75.0 jit_solution(17543464123038024076)
XLA Ops:
  0.6 71.8 %step.1 = (bf16[256,1024]{1,0:T(8,128)(2,1)}, f32[2,2,16,16,128]{4,3,2,1,0:T(8,128)}, f32[4,32,128]{2,1,0:T(8,128)}, f32[2,8,128]{2,1,0:T(8,128)}) custom-call(bf16[256,1024]{1,0:T(8,128)(2,1)} %x_ref.1, bf16[256,1024]{1,0:T(8,128)(2,1)} %c_ref.1, bf16[32,2048]{1,0:T(8,128)(2,1)} %u_ref.1, bf16[32,2048]{1,0:T(8,128)(2,1)} %bitcast.3), custom_call_target="tpu_custom_call" | custom-call | tf_op jit(solution)/shard_map/step/pallas_call | solution.py:686
  72.5 2.3 %layout.1 = (bf16[256,1024]{1,0:T(8,128)(2,1)}, f32[32,2048]{1,0:T(8,128)}, f32[32,2048]{1,0:T(8,128)}, f32[32]{0:T(128)}, f32[2,8,128]{2,1,0:T(8,128)}) custom-call(bf16[256,1024]{1,0:T(8,128)(2,1)} %get-tuple-element.14.gin_ref, f32[2,2,16,16,128]{4,3,2,1,0:T(8,128)} %get-tuple-element.15.grad_ref, f32[4,32,128]{2,1,0:T(8,128)} %get-tuple-element.16.eup_ref, ...), custom_call_target="tpu_custom_call" | custom-call | tf_op jit(solution)/shard_map/layout/pallas_call | solution.py:735

commit v5 on v4

--- a/solution.py
+++ b/solution.py
@@ -129,8 +129,8 @@
     c_ref,
     u_ref,
     d_ref,
-    gin_ref,
-    grad_ref,
+    gin,
+    outs,
     eup_ref,
     edn_ref,
     tok,
@@ -148,8 +148,6 @@
     pair_in,
     twin_out,
     twin_in,
-    outs,
-    gin,
     ebuf,
     eup,
     load_s,
@@ -164,7 +162,6 @@
     e_r,
     eu_r,
     sent,
-    out_s,
 ):
     rep, fs, tp = lax.axis_index("rep"), lax.axis_index("fs"), lax.axis_index("tp")
     mine = bits_of(fs)
@@ -505,11 +502,6 @@
         outs[m, rep, pl.ds(p * SIZE, SIZE)] = value
         return value
 
-    def output(i, src, dst):
-        copy = pltpu.make_async_copy(src, dst, out_s.at[i])
-        copy.start()
-        return copy
-
     rounds = ((near[3], near[4], far_x), (near[1], near[2], far_y), (near[0], twin, pair))
 
     def energy_copy(k, i):
@@ -526,7 +518,6 @@
 
     squares = [jnp.zeros((16, 128), f32), jnp.zeros((16, 128), f32)]
     left = [PARTS, PARTS]
-    outputs = []
     row_copies = []
 
     def arrived(m, p, k):
@@ -579,20 +570,15 @@
         s = slice(q * chunk, (q + 1) * chunk)
         scale = pair_in[q, 0:16].astype(f32)[0:1]
         gin[s] = (pre[s] + decode(pair_in[q, 16 : 16 + chunk], scale)).astype(bf16)
-        if q == pieces - 1:
-            outputs.append(output(0, gin, gin_ref))
 
     def energy_end():
         wait_bytes(ebuf.at[2, pl.ds(1, 3)], e_r.at[2])
-        ebuf[3, 0] = (ebuf[2, 0] + ebuf[2, 1]) * (1.0 / width)
-        ebuf[3, 1] = (ebuf[2, 2] + ebuf[2, 3]) * (1.0 / width)
-        outputs.append(output(2, ebuf.at[3, 0], edn_ref.at[rep]))
-        outputs.append(output(3, ebuf.at[3, 1], edn_ref.at[1 - rep]))
+        edn_ref[rep] = (ebuf[2, 0] + ebuf[2, 1]) * (1.0 / width)
+        edn_ref[1 - rep] = (ebuf[2, 2] + ebuf[2, 3]) * (1.0 / width)
 
     def twins_arrived(m):
         for g in (0,) if m == 1 else (1, 2):
             twin_receive(g)
-        outputs.append(output(4 if m == 0 else 1, outs.at[m], grad_ref.at[m]))
 
     def run(a):
         if a < 200:
@@ -621,7 +607,7 @@
     for a in THEN[-3:]:
         run(a)
     wait_bytes(eup.at[pl.ds(1, 3)], eu_r.at[0])
-    outputs.append(output(5, eup, eup_ref))
+    eup_ref[...] = (eup[0] + eup[1]) + (eup[2] + eup[3])
     wait_bytes(tok.at[:, pl.ds(0, rows)], sent.at[0])
     wait_bytes(tok.at[:, pl.ds(0, rows)], sent.at[1])
     wait_bytes(tok.at[:, pl.ds(0, rows)], sent.at[2])
@@ -633,18 +619,9 @@
     wait_bytes(ebuf.at[pl.ds(0, 3), pl.ds(0, 3)], sent.at[8])
     wait_bytes(eup.at[pl.ds(0, 3)], sent.at[9])
     wait_bytes(twin_out, sent.at[10])
-    for copy in outputs:
-        copy.wait()
-
-
-def layout(
-    gin_ref, grad_ref, eup_ref, edn_ref, gin_out, gup_out, gdn_out, eup_out, edn_out,
-    gin, grad, eup, edn, both, row, in_s, out_s,
-):
-    pairs = ((gin_ref, gin), (grad_ref.at[1], grad.at[1]), (grad_ref.at[0], grad.at[0]), (eup_ref, eup), (edn_ref, edn))
-    loads = [pltpu.make_async_copy(a, b, in_s.at[i]) for i, (a, b) in enumerate(pairs)]
-    for copy in loads:
-        copy.start()
+
+
+def layout(gin, grad, eup, edn, gin_out, gup_out, gdn_out, eup_out, edn_out, both, row, out_s):
     stores = []
 
     def store(i, src, dst):
@@ -653,22 +630,17 @@
         stores.append(copy)
 
     half = gup_out.shape[1] // 2
-    loads[3].wait()
-    total = (eup[0] + eup[1]) + (eup[2] + eup[3])
-    row[...] = jnp.sum(total.T, axis=0) * (1.0 / (4 * half))
-    loads[4].wait()
-    store(3, row, eup_out)
-    store(4, edn, edn_out)
-    loads[0].wait()
     store(0, gin, gin_out)
-    for m, load, out in ((1, 1, gdn_out), (0, 2, gup_out)):
-        loads[load].wait()
+    store(1, edn, edn_out)
+    for m, out in ((1, gdn_out), (0, gup_out)):
         for r in range(2):
             for u in range(UNITS):
                 block, top = divmod(u, 2)
                 left = r * half + block * 128
                 both[m, top * 16 : top * 16 + 16, left : left + 128] = grad[m, r, u]
-        store(load, both.at[m], out)
+        store(2 + m, both.at[m], out)
+    row[...] = jnp.sum(eup[...].T, axis=0) * (1.0 / (4 * half))
+    store(4, row, eup_out)
     for copy in stores:
         copy.wait()
 
@@ -683,16 +655,17 @@
     dma = pltpu.SemaphoreType.DMA
     messages = 2 * PARTS * ROOM
     anywhere = pl.BlockSpec(memory_space=pl.ANY)
+    vmem = pl.BlockSpec(memory_space=pltpu.VMEM)
     raw = pl.pallas_call(
         functools.partial(kernel, factor),
         out_shape=(
-            shape((rows, width), bf16),
-            shape((2, 2, UNITS, 16, 128), f32),
-            shape((4, shard, 128), f32),
-            shape((2, BLOCKS, 128), f32),
+            pltpu.VMEM((rows, width), bf16),
+            pltpu.VMEM((2, 2, UNITS, 16, 128), f32),
+            pltpu.VMEM((shard, 128), f32),
+            pltpu.VMEM((2, BLOCKS, 128), f32),
         ),
         in_specs=[anywhere] * 4,
-        out_specs=(anywhere,) * 4,
+        out_specs=(vmem,) * 4,
         scratch_shapes=[
             pltpu.VMEM((2, 4 * rows, width), bf16),
             pltpu.VMEM((2, width, 4 * rows), bf16),
@@ -709,8 +682,6 @@
             pltpu.VMEM((2, 16 + rows // 2, width), bf16),
             pltpu.VMEM((35, 16, 128), bf16),
             pltpu.VMEM((35, 16, 128), bf16),
-            pltpu.VMEM((2, 2, UNITS, 16, 128), f32),
-            pltpu.VMEM((rows, width), bf16),
             pltpu.VMEM((4, 4, BLOCKS, 128), f32),
             pltpu.VMEM((4, shard, 128), f32),
             dma((4,)),
@@ -725,7 +696,6 @@
             dma((3,)),
             dma((1,)),
             dma((11,)),
-            dma((6,)),
         ],
         compiler_params=pltpu.CompilerParams(
             collective_id=0, has_side_effects=True, vmem_limit_bytes=60 * 2**20
@@ -741,18 +711,14 @@
             shape((shard,), f32),
             shape((2, BLOCKS, 128), f32),
         ),
-        in_specs=[anywhere] * 4,
+        in_specs=[vmem] * 4,
         out_specs=(anywhere,) * 5,
         scratch_shapes=[
-            pltpu.VMEM((rows, width), bf16),
-            pltpu.VMEM((2, 2, UNITS, 16, 128), f32),
-            pltpu.VMEM((4, shard, 128), f32),
-            pltpu.VMEM((2, BLOCKS, 128), f32),
             pltpu.VMEM((2, shard, both), f32),
             pltpu.VMEM((shard,), f32),
             dma((5,)),
-            dma((5,)),
         ],
+        compiler_params=pltpu.CompilerParams(vmem_limit_bytes=8 * 2**20),
         name="layout",
     )(*raw)
     return gin, gup, gdn.T, eup, edn.reshape((both,))

time: 75.7 us -> 73.5 us (0.971)
  Pallas kernels: 74.2 us -> 72 us
    pallas_call x1, Pallas kernels: 2.33 us -> 1.01 us  [body(): pl.pallas_call(layout, out_shape=(shape((rows, width), bf16), shape((shar...]
    pallas_call x1, Pallas kernels: 71.8 us -> 71 us  [body(): pl.pallas_call(functools.partial(kernel, factor), out_shape=(pltpu.VMEM((...]
where the time goes in v5:
time: 73.5 us; the launch traced here: 72.8 us
  Pallas kernels  72 us (98%)
  between operations  0.82 us (1%)
    pallas_call x1, Pallas kernels, body(): pl.pallas_call(functools.partial(kernel, factor), out_shape=(pltpu.VMEM((...  71 us

profile of v5, /device:TPU:0, one launch (start us, length us, event | category | flops | bytes accessed | tf_op | source)
XLA Modules:
  0.0 72.8 jit_solution(11964621994424338179)
XLA Ops:
  0.6 71.0 %step.1 = (bf16[256,1024]{1,0:T(8,128)(2,1)S(1)}, f32[2,2,16,16,128]{4,3,2,1,0:T(8,128)S(1)}, f32[32,128]{1,0:T(8,128)S(1)}, f32[2,8,128]{2,1,0:T(8,128)S(1)}) custom-call(bf16[256,1024]{1,0:T(8,128)(2,1)} %x_ref.1, bf16[256,1024]{1,0:T(8,128)(2,1)} %c_ref.1, bf16[32,2048]{1,0:T(8,128)(2,1)} %u_ref.1, bf16[32,2048]{1,0:T(8,128)(2,1)} %bitcast.3), custom_call_target="tpu_custom_call" | custom-call | tf_op jit(solution)/shard_map/step/pallas_call | solution.py:659
  71.7 1.0 %layout.1 = (bf16[256,1024]{1,0:T(8,128)(2,1)}, f32[32,2048]{1,0:T(8,128)}, f32[32,2048]{1,0:T(8,128)}, f32[32]{0:T(128)}, f32[2,8,128]{2,1,0:T(8,128)}) custom-call(bf16[256,1024]{1,0:T(8,128)(2,1)S(1)} %get-tuple-element.14.gin, f32[2,2,16,16,128]{4,3,2,1,0:T(8,128)S(1)} %get-tuple-element.15.grad, f32[32,128]{1,0:T(8,128)S(1)} %get-tuple-element.16.eup, ...), custom_call_target="tpu_custom_call" | custom-call | tf_op jit(solution)/shard_map/layout/pallas_call | solution.py:705

commit v6 on v5

--- a/solution.py
+++ b/solution.py
@@ -65,7 +65,7 @@
     122, 20, 151, 40, 1301, 50, 112, 60, 30, 70, 142, 162, 1300, 132, 11, 172,
     1, 103, 152, 21, 123, 41, 51, 113, 31, 61, 71, 143, 163, 12, 133, 173,
     2, 22, 153, 42, 52, 32, 72, 62, 13, 3, 1400, 23, 43, 1500, 53, 33,
-    73, 63, 1401, 1402, 1310, 1311,
+    73, 63, 1401, 1310, 1311, 1402,
 )
 STEPS = 5
 PARTS = 8
@@ -502,18 +502,30 @@
         outs[m, rep, pl.ds(p * SIZE, SIZE)] = value
         return value
 
-    rounds = ((near[3], near[4], far_x), (near[1], near[2], far_y), (near[0], twin, pair))
+    rounds = ((near[0], twin, pair), (near[3], near[4], far_x), (near[1], near[2], far_y))
 
     def energy_copy(k, i):
-        return remote(ebuf.at[k, 0], ebuf.at[k, 1 + i], sent.at[8], e_r.at[k], rounds[k][i])
+        n = 1 if k == 0 else 2
+        return remote(
+            ebuf.at[k, 0, pl.ds(0, n)],
+            ebuf.at[k, 1 + i, pl.ds(0, n)],
+            sent.at[11 if k == 0 else 8],
+            e_r.at[k],
+            rounds[k][i],
+        )
 
     def energy_begin(k):
         for i in range(3):
             start(energy_copy(k, i))
 
     def energy_step(k):
-        wait_bytes(ebuf.at[k, pl.ds(1, 3)], e_r.at[k])
-        ebuf[k + 1, 0] = (ebuf[k, 0] + ebuf[k, 1]) + (ebuf[k, 2] + ebuf[k, 3])
+        if k == 0:
+            wait_bytes(ebuf.at[0, pl.ds(1, 3), 0], e_r.at[0])
+            ebuf[1, 0, 0] = ebuf[0, 0, 0] + ebuf[0, 1, 0]
+            ebuf[1, 0, 1] = ebuf[0, 2, 0] + ebuf[0, 3, 0]
+        else:
+            wait_bytes(ebuf.at[k, pl.ds(1, 3)], e_r.at[k])
+            ebuf[k + 1, 0] = (ebuf[k, 0] + ebuf[k, 1]) + (ebuf[k, 2] + ebuf[k, 3])
         energy_begin(k + 1)
 
     squares = [jnp.zeros((16, 128), f32), jnp.zeros((16, 128), f32)]
@@ -528,7 +540,7 @@
         left[m] -= 1
         if m == 1:
             total = value[0] * value[0] + value[1] * value[1]
-            ebuf[0, 0, p : p + 1, :] = jnp.sum(total, axis=0, keepdims=True)
+            ebuf[0, 0, 0, p : p + 1, :] = jnp.sum(total, axis=0, keepdims=True)
             if left[m] == 0:
                 energy_begin(0)
                 twin_send(0)
@@ -573,8 +585,9 @@
 
     def energy_end():
         wait_bytes(ebuf.at[2, pl.ds(1, 3)], e_r.at[2])
-        edn_ref[rep] = (ebuf[2, 0] + ebuf[2, 1]) * (1.0 / width)
-        edn_ref[1 - rep] = (ebuf[2, 2] + ebuf[2, 3]) * (1.0 / width)
+        total = (ebuf[2, 0] + ebuf[2, 1]) + (ebuf[2, 2] + ebuf[2, 3])
+        edn_ref[rep] = total[0] * (1.0 / width)
+        edn_ref[1 - rep] = total[1] * (1.0 / width)
 
     def twins_arrived(m):
         for g in (0,) if m == 1 else (1, 2):
@@ -601,10 +614,10 @@
         else:
             twins_arrived(1)
 
-    for a in THEN[:-3]:
+    for a in THEN[:-1]:
         run(a)
     twins_arrived(0)
-    for a in THEN[-3:]:
+    for a in THEN[-1:]:
         run(a)
     wait_bytes(eup.at[pl.ds(1, 3)], eu_r.at[0])
     eup_ref[...] = (eup[0] + eup[1]) + (eup[2] + eup[3])
@@ -616,7 +629,8 @@
     wait_bytes(sbuf, sent.at[5])
     wait_bytes(part_in, sent.at[6])
     wait_bytes(pair_out, sent.at[7])
-    wait_bytes(ebuf.at[pl.ds(0, 3), pl.ds(0, 3)], sent.at[8])
+    wait_bytes(ebuf.at[0, pl.ds(0, 3), 0], sent.at[11])
+    wait_bytes(ebuf.at[pl.ds(1, 2), pl.ds(0, 3)], sent.at[8])
     wait_bytes(eup.at[pl.ds(0, 3)], sent.at[9])
     wait_bytes(twin_out, sent.at[10])
 
@@ -682,7 +696,7 @@
             pltpu.VMEM((2, 16 + rows // 2, width), bf16),
             pltpu.VMEM((35, 16, 128), bf16),
             pltpu.VMEM((35, 16, 128), bf16),
-            pltpu.VMEM((4, 4, BLOCKS, 128), f32),
+            pltpu.VMEM((3, 4, 2, BLOCKS, 128), f32),
             pltpu.VMEM((4, shard, 128), f32),
             dma((4,)),
             dma((2, 4)),
@@ -695,7 +709,7 @@
             dma((2,)),
             dma((3,)),
             dma((1,)),
-            dma((11,)),
+            dma((12,)),
         ],
         compiler_params=pltpu.CompilerParams(
             collective_id=0, has_side_effects=True, vmem_limit_bytes=60 * 2**20

time: 73.5 us -> 77.5 us (1.054)
  Pallas kernels: 72 us -> 76.6 us
    pallas_call x1, Pallas kernels: 71 us -> 75.6 us  [body(): pl.pallas_call(functools.partial(kernel, factor), out_shape=(pltpu.VMEM((...]
where the time goes in v6:
time: 77.5 us; the launch traced here: 77.4 us
  Pallas kernels  76.6 us (99%)
  between operations  0.82 us (1%)
    pallas_call x1, Pallas kernels, body(): pl.pallas_call(functools.partial(kernel, factor), out_shape=(pltpu.VMEM((...  75.6 us

profile of v6, /device:TPU:0, one launch (start us, length us, event | category | flops | bytes accessed | tf_op | source)
XLA Modules:
  0.0 77.4 jit_solution(1337775468533946850)
XLA Ops:
  0.6 75.6 %step.1 = (bf16[256,1024]{1,0:T(8,128)(2,1)S(1)}, f32[2,2,16,16,128]{4,3,2,1,0:T(8,128)S(1)}, f32[32,128]{1,0:T(8,128)S(1)}, f32[2,8,128]{2,1,0:T(8,128)S(1)}) custom-call(bf16[256,1024]{1,0:T(8,128)(2,1)} %x_ref.1, bf16[256,1024]{1,0:T(8,128)(2,1)} %c_ref.1, bf16[32,2048]{1,0:T(8,128)(2,1)} %u_ref.1, bf16[32,2048]{1,0:T(8,128)(2,1)} %bitcast.3), custom_call_target="tpu_custom_call" | custom-call | tf_op jit(solution)/shard_map/step/pallas_call | solution.py:673
  76.2 1.0 %layout.1 = (bf16[256,1024]{1,0:T(8,128)(2,1)}, f32[32,2048]{1,0:T(8,128)}, f32[32,2048]{1,0:T(8,128)}, f32[32]{0:T(128)}, f32[2,8,128]{2,1,0:T(8,128)}) custom-call(bf16[256,1024]{1,0:T(8,128)(2,1)S(1)} %get-tuple-element.14.gin, f32[2,2,16,16,128]{4,3,2,1,0:T(8,128)S(1)} %get-tuple-element.15.grad, f32[32,128]{1,0:T(8,128)S(1)} %get-tuple-element.16.eup, ...), custom_call_target="tpu_custom_call" | custom-call | tf_op jit(solution)/shard_map/layout/pallas_call | solution.py:719

commit v7 on v5

--- a/solution.py
+++ b/solution.py
@@ -64,8 +64,8 @@
     170, 150, 101, 1002, 111, 121, 1003, 131, 141, 1201, 0, 161, 10, 171, 102, 1200,
     122, 20, 151, 40, 1301, 50, 112, 60, 30, 70, 142, 162, 1300, 132, 11, 172,
     1, 103, 152, 21, 123, 41, 51, 113, 31, 61, 71, 143, 163, 12, 133, 173,
-    2, 22, 153, 42, 52, 32, 72, 62, 13, 3, 1400, 23, 43, 1500, 53, 33,
-    73, 63, 1401, 1402, 1310, 1311,
+    2, 22, 153, 42, 52, 32, 72, 62, 13, 3, 1400, 23, 43, 53, 33, 73,
+    63, 1401, 1500, 1310, 1311, 1402,
 )
 STEPS = 5
 PARTS = 8
@@ -601,10 +601,10 @@
         else:
             twins_arrived(1)
 
-    for a in THEN[:-3]:
+    for a in THEN[:-1]:
         run(a)
     twins_arrived(0)
-    for a in THEN[-3:]:
+    for a in THEN[-1:]:
         run(a)
     wait_bytes(eup.at[pl.ds(1, 3)], eu_r.at[0])
     eup_ref[...] = (eup[0] + eup[1]) + (eup[2] + eup[3])

time: 73.5 us -> 73.3 us (level)
  no operation moved by 1% of the time
where the time goes in v7:
time: 73.3 us; the launch traced here: 72.7 us
  Pallas kernels  71.9 us (98%)
  between operations  0.82 us (1%)
    pallas_call x1, Pallas kernels, body(): pl.pallas_call(functools.partial(kernel, factor), out_shape=(pltpu.VMEM((...  70.8 us

profile of v7, /device:TPU:0, one launch (start us, length us, event | category | flops | bytes accessed | tf_op | source)
XLA Modules:
  0.0 72.7 jit_solution(9079015404626072401)
XLA Ops:
  0.6 70.8 %step.1 = (bf16[256,1024]{1,0:T(8,128)(2,1)S(1)}, f32[2,2,16,16,128]{4,3,2,1,0:T(8,128)S(1)}, f32[32,128]{1,0:T(8,128)S(1)}, f32[2,8,128]{2,1,0:T(8,128)S(1)}) custom-call(bf16[256,1024]{1,0:T(8,128)(2,1)} %x_ref.1, bf16[256,1024]{1,0:T(8,128)(2,1)} %c_ref.1, bf16[32,2048]{1,0:T(8,128)(2,1)} %u_ref.1, bf16[32,2048]{1,0:T(8,128)(2,1)} %bitcast.3), custom_call_target="tpu_custom_call" | custom-call | tf_op jit(solution)/shard_map/step/pallas_call | solution.py:659
  71.5 1.0 %layout.1 = (bf16[256,1024]{1,0:T(8,128)(2,1)}, f32[32,2048]{1,0:T(8,128)}, f32[32,2048]{1,0:T(8,128)}, f32[32]{0:T(128)}, f32[2,8,128]{2,1,0:T(8,128)}) custom-call(bf16[256,1024]{1,0:T(8,128)(2,1)S(1)} %get-tuple-element.14.gin, f32[2,2,16,16,128]{4,3,2,1,0:T(8,128)S(1)} %get-tuple-element.15.grad, f32[32,128]{1,0:T(8,128)S(1)} %get-tuple-element.16.eup, ...), custom_call_target="tpu_custom_call" | custom-call | tf_op jit(solution)/shard_map/layout/pallas_call | solution.py:705
